TPU v7x, 32 devices: a whole 2x2x4 slice. The times are simulated.
32 devices in a mesh: fs: 16 (over z, y, x), tp: 2 (over core).
Axes of the slice: x: 2, y: 2, z: 4, core: 2. Of those that a mesh axis runs over, the one named last changes fastest.
Arguments:
- layer_input: bfloat16 [16384, 2048], P('fs'), may hold values from -6 to 6
- value_cotangent: bfloat16 [16384, 1024], P('fs', 'tp'), may hold values from -0.046875 to 0.046875
- mixed_output: bfloat16 [16384, 1024], P('fs'), may hold values from -6 to 6
- output_cotangent: bfloat16 [16384, 2048], P('fs', 'tp'), may hold values from -0.046875 to 0.046875
- value_weight: float32 [2048, 1024], P('fs', 'tp'), may hold values from -0.125 to 0.125
- out_weight: float32 [1024, 2048], P('fs', 'tp'), may hold values from -0.1875 to 0.1875
- value_basis: bfloat16 [2048, 256], P('fs'), may hold values from -0.125 to 0.125
- out_basis: bfloat16 [1024, 256], P('fs'), may hold values from -0.1875 to 0.1875
- value_first: float32 [256, 1024], P('fs', 'tp'), may hold values from -6 to 6
- value_second: float32 [256, 1024], P('fs', 'tp'), may hold values from 0.5 to 2
- out_first: float32 [256, 2048], P('fs', 'tp'), may hold values from -6 to 6
- out_second: float32 [256, 2048], P('fs', 'tp'), may hold values from 0.5 to 2
Outputs:
- value_new: float32 [2048, 1024], P('fs', 'tp')
- out_new: float32 [1024, 2048], P('fs', 'tp')
- value_step: float32 [2048, 1024], P('fs', 'tp')
- out_step: float32 [1024, 2048], P('fs', 'tp')
- value_copy: bfloat16 [2048, 1024], P(None, 'tp')
- out_copy: bfloat16 [1024, 2048], P(None, 'tp')
- value_first_new: float32 [256, 1024], P('fs', 'tp')
- value_second_new: float32 [256, 1024], P('fs', 'tp')
- out_first_new: float32 [256, 2048], P('fs', 'tp')
- out_second_new: float32 [256, 2048], P('fs', 'tp')
All inputs are finite; a program needn't handle non-finite values.
Results may differ from a plain program's by a relative error of at most 0.00045.
Values may be sent and summed in bfloat16 or wider, within the bound.
A program may use at most 64 MiB of HBM per device.

v0:
```python
import jax
import jax.numpy as jnp
from jax import lax
from jax.sharding import PartitionSpec as P

D = 2048
W = 1024
R = 256


first_decay = 0.8
second_decay = 0.9
step_rate = 0.1


def contract(left, right, precision=None):
    return lax.dot_general(
        left,
        right,
        (((0,), (0,)), ((), ())),
        preferred_element_type=jnp.float32,
        precision=precision,
    )


def moments(projected, first, second):
    first_new = first_decay * first + (1.0 - first_decay) * projected
    second_new = second_decay * second + (1.0 - second_decay) * projected * projected
    return (first_new, second_new, first_new / jnp.sqrt(second_new))


def split_parts(wide):
    upper = wide.astype(jnp.bfloat16)
    upper_back = lax.optimization_barrier(upper).astype(jnp.float32)
    lower = (wide - upper_back).astype(jnp.bfloat16)
    return (upper, lower)


def local(
    layer_input,
    value_cotangent,
    mixed_output,
    output_cotangent,
    value_weight,
    out_weight,
    value_basis,
    out_basis,
    value_first,
    value_second,
    out_first,
    out_second,
):
    highest = lax.Precision.HIGHEST
    value_cols = value_cotangent.shape[1]

    def reduce_rows(source, piece):
        return jnp.dot(source, piece, preferred_element_type=jnp.float32)

    value_reduced = reduce_rows(layer_input, lax.all_gather(value_basis, "fs", axis=0, tiled=True))
    out_reduced = reduce_rows(mixed_output, lax.all_gather(out_basis, "fs", axis=0, tiled=True))
    value_upper, value_lower = split_parts(value_reduced)
    out_upper, out_lower = split_parts(out_reduced)
    value_part = contract(value_upper, value_cotangent) + contract(value_lower, value_cotangent)
    out_part = contract(out_upper, output_cotangent) + contract(out_lower, output_cotangent)
    projected = lax.psum_scatter(
        jnp.concatenate([value_part, out_part], axis=1), "fs", scatter_dimension=0, tiled=True
    )
    value_first_new, value_second_new, value_dir = moments(
        projected[:, :value_cols], value_first, value_second
    )
    out_first_new, out_second_new, out_dir = moments(
        projected[:, value_cols:], out_first, out_second
    )
    local_total = jnp.sum(value_dir * value_dir) + jnp.sum(out_dir * out_dir)
    total = lax.psum(local_total, ("fs", "tp"))
    scale = step_rate / jnp.sqrt(1.0 + total / (R * (W + D)))
    basis_value = value_basis.astype(jnp.float32)
    basis_out = out_basis.astype(jnp.float32)
    value_sum = jnp.dot(
        basis_value, lax.all_gather(value_dir, "fs", axis=0, tiled=True), precision=highest
    )
    out_sum = jnp.dot(
        basis_out, lax.all_gather(out_dir, "fs", axis=0, tiled=True), precision=highest
    )
    value_step = scale * value_sum
    out_step = scale * out_sum
    value_new = value_weight - value_step
    out_new = out_weight - out_step
    value_copy, out_copy = (
        lax.all_gather(value_new.astype(jnp.bfloat16), "fs", axis=0, tiled=True),
        lax.all_gather(out_new.astype(jnp.bfloat16), "fs", axis=0, tiled=True),
    )
    return (
        value_new,
        out_new,
        value_step,
        out_step,
        value_copy,
        out_copy,
        value_first_new,
        value_second_new,
        out_first_new,
        out_second_new,
    )


def solution(mesh):
    placed = (
        P("fs", None),
        P("fs", "tp"),
        P("fs", None),
        P("fs", "tp"),
        P("fs", "tp"),
        P("fs", "tp"),
        P("fs", None),
        P("fs", None),
        P("fs", "tp"),
        P("fs", "tp"),
        P("fs", "tp"),
        P("fs", "tp"),
    )
    return jax.shard_map(
        local,
        mesh=mesh,
        in_specs=placed,
        out_specs=(
            P("fs", "tp"),
            P("fs", "tp"),
            P("fs", "tp"),
            P("fs", "tp"),
            P(None, "tp"),
            P(None, "tp"),
            P("fs", "tp"),
            P("fs", "tp"),
            P("fs", "tp"),
            P("fs", "tp"),
        ),
        check_vma=False,
    )
```

profile of v0, /device:TPU:0, one launch (start us, length us, event | category | flops | bytes accessed | tf_op | source)
XLA Modules:
  0.0 420.3 jit_solution(7661621725314440881)
XLA Ops:
  7.2 0.0 all-gather.5.cloned.1.call-start
  7.2 0.7 all-gather.5.cloned.1.call-update
  7.9 0.0 reduce-scatter.2.cloned.1.call-start
  8.0 45.9 %all_gather.19 = bf16[1024,256]{1,0:T(8,128)(2,1)S(1)} all-gather(bf16[64,256]{1,0:T(8,128)(2,1)} %param.19), channel_id=1, replica_groups=mesh['fs'=16,'tp'=2] {'fs'}, dimensions={0}, use_global_device_ids=true | all-gather | bytes 557056 | tf_op jit(solution)/shard_map/all_gather | solution.py:60
  53.9 0.7 fusion.8
  54.6 1.0 copy-done.1
  55.6 0.7 fusion.11
  56.4 1.7 convolution_add_fusion
  58.1 10.8 %all-gather.5.cloned.1.call-done = bf16[2048,256]{1,0:T(8,128)(2,1)} async-done(((bf16[128,256]{1,0:T(8,128)(2,1)}), bf16[2048,256]{1,0:T(8,128)(2,1)}) %all-gather.5.cloned.1.call-update) | async-done | bytes 1048592 | tf_op jit(solution)/shard_map/all_gather | solution.py:59
  68.9 3.7 fusion.9
  72.6 0.4 fusion.10
  73.1 0.5 convolution_add_fusion.1
  73.6 0.7 copy-done.3
  74.4 1.3 pad_maximum_fusion
  75.7 0.0 all-gather.7.cloned.1.call-start
  75.7 125.0 %reduce-scatter.2.cloned.1.call-done = f32[16,1536]{1,0:T(8,128)} async-done(((f32[256,1536]{1,0:T(8,128)}), f32[16,1536]{1,0:T(8,128)}) %reduce-scatter.2.cloned.1.call-update) | async-done | bytes 98320 | tf_op jit(solution)/shard_map/reduce_scatter | solution.py:65
  200.7 2.1 multiply_reduce_fusion
  202.8 0.0 all-gather.9.cloned.1.call-start
  202.9 2.0 multiply_reduce_fusion.1
  206.2 0.1 copy.22
  206.4 40.1 %psum.7 = f32[]{:T(128)} all-reduce(f32[]{:T(128)S(6)} %add.31), channel_id=1, replica_groups=mesh['fs'=16,'tp'=2] {'fs','tp'}, use_global_device_ids=true, to_apply=%region_3.0 | all-reduce | flops 1 | bytes 8 | tf_op jit(solution)/shard_map/psum | solution.py:75
  247.2 42.0 %all_gather.20 = f32[256,512]{1,0:T(8,128)S(1)} all-gather(f32[16,512]{1,0:T(8,128)S(1)} %get-tuple-element.29), channel_id=1, replica_groups=mesh['fs'=16,'tp'=2] {'fs'}, dimensions={0}, use_global_device_ids=true | all-gather | bytes 557056 | tf_op jit(solution)/shard_map/all_gather | solution.py:80
  289.2 1.3 fusion.5
  290.5 0.0 all-gather.11.cloned.1.call-start
  290.5 0.0 all-gather.7.cloned.1.call-done
  290.6 2.6 fusion.4
  293.2 0.8 copy.23
  294.0 0.8 copy.24
  294.8 54.6 %all-gather.9.cloned.1.call-done = bf16[2048,512]{0,1:T(8,128)(2,1)} async-done(((bf16[128,512]{0,1:T(8,128)(2,1)}), bf16[2048,512]{0,1:T(8,128)(2,1)}) %all-gather.9.cloned.1.call-update) | async-done | bytes 2097168 | tf_op jit(solution)/shard_map/all_gather | solution.py:90
  349.4 3.9 copy.25
  353.4 57.3 %all-gather.11.cloned.1.call-done = bf16[1024,1024]{1,0:T(8,128)(2,1)} async-done(((bf16[64,1024]{1,0:T(8,128)(2,1)}), bf16[1024,1024]{1,0:T(8,128)(2,1)}) %all-gather.11.cloned.1.call-update) | async-done | bytes 2097168 | tf_op jit(solution)/shard_map/all_gather | solution.py:91
  410.7 3.1 copy.27
  (26 shorter events, 0.1 us)
Async XLA Ops:
  7.2 46.7 %copy-start = (bf16[1024,1024]{1,0:T(8,128)(2,1)S(1)}, bf16[1024,1024]{1,0:T(8,128)(2,1)}, u32[]{:S(2)}) copy-start(bf16[1024,1024]{1,0:T(8,128)(2,1)} %param.14) | copy-start | bytes 6291460
  7.2 61.7 %all-gather.5.cloned.1.call-start = ((), (), s32[]{:S(2)}) async-start(), calls=%async_computation.1 | async-start | bytes 1114112 | tf_op jit(solution)/shard_map/all_gather | solution.py:59
  7.9 192.8 %reduce-scatter.2.cloned.1.call-start = ((), (), s32[]{:S(2)}) async-start(), calls=%async_computation.2 | async-start | bytes 1671168 | tf_op jit(solution)/shard_map/reduce_scatter | solution.py:65
  53.9 1.7 copy-start.1
  58.1 14.6 %copy-start.2 = (bf16[1024,512]{1,0:T(8,128)(2,1)S(1)}, bf16[1024,512]{1,0:T(8,128)(2,1)}, u32[]{:S(2)}) copy-start(bf16[1024,512]{1,0:T(8,128)(2,1)} %param.13) | copy-start | bytes 3145732
  73.1 1.2 copy-start.3
  74.3 126.4 %copy-start.8 = (f32[16,1024]{1,0:T(8,128)S(1)}, f32[16,1024]{1,0:T(8,128)}, u32[]{:S(2)}) copy-start(f32[16,1024]{1,0:T(8,128)} %param.23) | copy-start | bytes 196612
  74.3 126.4 %copy-start.9 = (f32[16,1024]{1,0:T(8,128)S(1)}, f32[16,1024]{1,0:T(8,128)}, u32[]{:S(2)}) copy-start(f32[16,1024]{1,0:T(8,128)} %param.22) | copy-start | bytes 196612
  74.3 128.6 %copy-start.10 = (f32[16,512]{1,0:T(8,128)S(1)}, f32[16,512]{1,0:T(8,128)}, u32[]{:S(2)}) copy-start(f32[16,512]{1,0:T(8,128)} %param.21) | copy-start | bytes 98308
  74.3 128.6 %copy-start.11 = (f32[16,512]{1,0:T(8,128)S(1)}, f32[16,512]{1,0:T(8,128)}, u32[]{:S(2)}) copy-start(f32[16,512]{1,0:T(8,128)} %param.20) | copy-start | bytes 98308
  74.3 131.9 %copy-start.6 = (f32[128,512]{1,0:T(8,128)S(1)}, f32[128,512]{1,0:T(8,128)}, u32[]{:S(2)}) copy-start(f32[128,512]{1,0:T(8,128)} %param.16) | copy-start | bytes 786436
  75.6 213.6 %copy-start.5 = (bf16[128,256]{1,0:T(8,128)(2,1)S(1)}, bf16[128,256]{1,0:T(8,128)(2,1)}, u32[]{:S(2)}) copy-start(bf16[128,256]{1,0:T(8,128)(2,1)} %param.18) | copy-start | bytes 196612
  75.6 214.9 %copy-start.4 = (f32[64,1024]{1,0:T(8,128)S(1)}, f32[64,1024]{1,0:T(8,128)}, u32[]{:S(2)}) copy-start(f32[64,1024]{1,0:T(8,128)} %param.17) | copy-start | bytes 786436
  75.6 214.9 %copy-start.7 = (bf16[64,256]{1,0:T(8,128)(2,1)S(1)}, bf16[64,256]{1,0:T(8,128)(2,1)}, u32[]{:S(2)}) copy-start(bf16[64,256]{1,0:T(8,128)(2,1)} %param.19) | copy-start | bytes 98308
  75.7 214.9 %all-gather.7.cloned.1.call-start = ((), (), s32[]{:S(2)}) async-start(), calls=%async_computation.3 | async-start | bytes 1114112 | tf_op jit(solution)/shard_map/all_gather | solution.py:83
  202.8 146.6 %all-gather.9.cloned.1.call-start = ((), (), s32[]{:S(2)}) async-start(), calls=%async_computation.4 | async-start | bytes 2228224 | tf_op jit(solution)/shard_map/all_gather | solution.py:90
  290.5 120.2 %all-gather.11.cloned.1.call-start = ((), (), s32[]{:S(2)}) async-start(), calls=%async_computation.5 | async-start | bytes 2228224 | tf_op jit(solution)/shard_map/all_gather | solution.py:91
Sparse Core Ops, SparseCore 0:
  10.8 58.0 all-gather.4
  75.8 124.8 reduce-scatter.1
  204.0 54.8 all-gather.6
  290.6 58.7 all-gather.8
  352.1 58.5 all-gather.10
where the time goes:
time: 421 us; the launch traced here: 420 us
  waiting for transfers between devices  248 us (59%)
  blocking collectives  128 us (30%)
  between operations  15.9 us (4%)
  matrix products  11.7 us (3%)
  local copies, waits for them, and re-layouts  10.6 us (3%)
  other arithmetic  5.39 us (1%)
    reduce_scatter x1, waiting for transfers between devices, local(): lax.psum_scatter(jnp.concatenate([value_part, out_part], axis=1), 'fs', s...  125 us
    all_gather x1, waiting for transfers between devices, local(): lax.all_gather(out_new.astype(jnp.bfloat16), 'fs', axis=0, tiled=True)  57.3 us
    all_gather x1, waiting for transfers between devices, local(): lax.all_gather(value_new.astype(jnp.bfloat16), 'fs', axis=0, tiled=True)  54.6 us
    all_gather x1, blocking collectives, local(): lax.all_gather(out_basis, 'fs', axis=0, tiled=True)  45.9 us
    all_gather x1, blocking collectives, local(): lax.all_gather(value_dir, 'fs', axis=0, tiled=True)  42 us
    psum x1, blocking collectives, local(): total = lax.psum(local_total, ('fs', 'tp'))  40.1 us
    all_gather x1, waiting for transfers between devices, local(): lax.all_gather(value_basis, 'fs', axis=0, tiled=True)  10.8 us
    unnamed x29, local copies, waits for them, and re-layouts  10.6 us
  transfers between devices with their start and end apart: 5, of which 4 were waited for; matrix products, arithmetic and copies ran while one was open for 4% of the time, Pallas kernels for 0%

commit v1 on v0

v1 whole, which is shorter than its diff:
```python
import functools
import itertools

import jax
import jax.numpy as jnp
from jax import lax
from jax.experimental import pallas as pl
from jax.experimental.pallas import tpu as pltpu
from jax.sharding import PartitionSpec as P

first_decay = 0.8
second_decay = 0.9
step_rate = 0.1


def split_digits(n):
    digits = []
    stride = 1
    for _ in range(2):
        if n % 2 == 0 and n > 2:
            digits.append((2, stride))
            stride *= 2
            n //= 2
    digits.append((n, stride))
    return digits


def orders_of(digits):
    slow, fast = digits[-1], digits[:-1]
    return [slow, *fast], [slow, *fast[::-1]]


def shifted(me, order, offsets, sign):
    out = me
    for (size, stride), off in zip(order, offsets):
        if off:
            digit = lax.rem(lax.div(me, stride), size)
            other = lax.rem(digit + (off if sign > 0 else size - off), size)
            out = out + (other - digit) * stride
    return out


def flat(order, offsets):
    out = 0
    for (size, _), off in zip(order, offsets):
        out = out * size + off
    return out


class Gather:
    def __init__(self, me, dst, order, send_sem, recv_sem):
        self.me, self.dst, self.order = me, dst, order
        self.send_sem, self.recv_sem = send_sem, recv_sem
        self.sent = []

    def copy(self, held, axis, off):
        target = tuple(off if i == axis else h for i, h in enumerate(held))
        slot = flat(self.order, target)
        block = shifted(self.me, self.order, held, -1)
        peer = shifted(self.me, self.order, tuple(off if i == axis else 0 for i in range(len(held))), 1)
        return pltpu.make_async_remote_copy(
            src_ref=self.dst.at[block],
            dst_ref=self.dst.at[block],
            send_sem=self.send_sem.at[slot],
            recv_sem=self.recv_sem.at[slot],
            device_id={"fs": peer},
            device_id_type=pl.DeviceIdType.MESH,
        )

    def forward(self, held):
        last = max([i for i, h in enumerate(held) if h], default=-1)
        for axis in range(last + 1, len(self.order)):
            for off in range(1, self.order[axis][0]):
                c = self.copy(held, axis, off)
                c.start()
                self.sent.append(c)

    def arrive(self, held):
        if any(held):
            slot = flat(self.order, held)
            block = shifted(self.me, self.order, held, -1)
            pltpu.make_async_remote_copy(
                src_ref=self.dst.at[block],
                dst_ref=self.dst.at[block],
                send_sem=self.send_sem.at[slot],
                recv_sem=self.recv_sem.at[slot],
                device_id={"fs": self.me},
                device_id_type=pl.DeviceIdType.MESH,
            ).wait_recv()

    def all_held(self):
        rows = list(itertools.product(*[range(s) for s, _ in self.order]))
        return sorted(rows, key=lambda h: max([i for i, v in enumerate(h) if v], default=-1))

    def drain(self):
        for c in self.sent:
            c.wait_send()


def gather_all(gathers, started=()):
    for steps in itertools.zip_longest(*[g.all_held() for g in gathers]):
        for g, held in zip(gathers, steps):
            if held is not None:
                g.arrive(held)
                g.forward(held)
    for g in gathers:
        g.drain()


class Scatter:
    def __init__(self, me, part, bufs, stage, order, send_sem, recv_sem):
        self.me, self.part, self.bufs, self.stage = me, part, bufs, stage
        self.order, self.send_sem, self.recv_sem = order, send_sem, recv_sem
        self.sent = []

    def slot(self, js):
        return flat(self.order, js)

    def copy(self, js):
        axis = next(i for i, j in enumerate(js) if j)
        slot = self.slot(js)
        peer = shifted(self.me, self.order, tuple(j if i == axis else 0 for i, j in enumerate(js)), 1)
        src = self.part.at[shifted(self.me, self.order, js, 1)] if axis == 0 else self.stage.at[slot]
        return pltpu.make_async_remote_copy(
            src_ref=src,
            dst_ref=self.bufs.at[slot],
            send_sem=self.send_sem.at[slot],
            recv_sem=self.recv_sem.at[slot],
            device_id={"fs": peer},
            device_id_type=pl.DeviceIdType.MESH,
        )

    def summed(self, js):
        axis = next((i for i, j in enumerate(js) if j), len(js))
        total = self.part[shifted(self.me, self.order, js, 1)]
        for i in range(axis):
            for off in range(1, self.order[i][0]):
                src = tuple(off if k == i else (js[k] if k > i else 0) for k in range(len(js)))
                self.copy(src).wait_recv()
                total = total + self.bufs[self.slot(src)]
        return total

    def tasks(self):
        rows = list(itertools.product(*[range(s) for s, _ in self.order]))
        first = lambda js: next((i for i, j in enumerate(js) if j), len(js))
        return sorted(rows, key=lambda js: (first(js), first(js[first(js) + 1:]) if first(js) < len(js) else 0))

    def run(self, js):
        if not any(js):
            return
        axis = next(i for i, j in enumerate(js) if j)
        if axis > 0:
            self.stage[self.slot(js)] = self.summed(js)
        c = self.copy(js)
        c.start()
        self.sent.append(c)

    def drain(self):
        for c in self.sent:
            c.wait_send()


def two_parts(wide):
    upper = wide.astype(jnp.bfloat16)
    lower = (wide - upper.astype(jnp.float32)).astype(jnp.bfloat16)
    return upper, lower


def dot(a, b, dims=(((1,), (0,)), ((), ()))):
    return lax.dot_general(a, b, dims, preferred_element_type=jnp.float32)


def merged(ref):
    n, r, c = ref.shape
    if r % 8 == 0:
        return ref[...].reshape(n * r, c)
    return jnp.concatenate([ref[i] for i in range(n)], axis=0)


def kernel(
    n, m, total_size,
    x_hbm, vc_hbm, mo_hbm, oc_hbm,
    vw, ow, vb, ob, vf, vs, of, os_,
    vnew, onew, vstep, ostep, vcopy, ocopy, vf_new, vs_new, of_new, os_new,
    x_ref, vc_ref, mo_ref, oc_ref,
    vb_all, ob_all, vpart, opart, vacc, oacc, vrs, ors, vstage, ostage, vdir, odir, squares,
    load_sem, g_send, g_recv, s_send, s_recv, q_send, q_recv,
):
    me = lax.axis_index("fs")
    mine = lax.axis_index("tp")
    digits = split_digits(n)
    order_a, order_b = orders_of(digits)

    loads = [
        pltpu.make_async_copy(src, dst, load_sem.at[i])
        for i, (src, dst) in enumerate(((x_hbm, x_ref), (vc_hbm, vc_ref), (mo_hbm, mo_ref), (oc_hbm, oc_ref)))
    ]
    for c in loads:
        c.start()
    vb_all[me] = vb[...]
    ob_all[me] = ob[...]

    barrier = pltpu.get_barrier_semaphore()
    peers = 0
    for size, stride in digits:
        for off in range(1, size):
            pl.semaphore_signal(
                barrier, inc=1, device_id={"fs": shifted(me, [(size, stride)], (off,), 1)},
                device_id_type=pl.DeviceIdType.MESH,
            )
            peers += 1
    for off in range(1, m):
        pl.semaphore_signal(
            barrier, inc=1, device_id={"tp": lax.rem(mine + off, m)},
            device_id_type=pl.DeviceIdType.MESH,
        )
        peers += 1
    pl.semaphore_wait(barrier, peers)

    gather_all([
        Gather(me, vb_all, order_a, g_send.at[0], g_recv.at[0]),
        Gather(me, ob_all, order_b, g_send.at[1], g_recv.at[1]),
    ])
    for c in loads:
        c.wait()

    tokens = x_ref.shape[0]
    tile = min(256, tokens)
    v_basis = merged(vb_all)
    o_basis = merged(ob_all)
    vacc[...] = jnp.zeros_like(vacc)
    oacc[...] = jnp.zeros_like(oacc)

    def project(src, cot, basis, acc):
        def body(t, carry):
            rows = pl.ds(pl.multiple_of(t * tile, tile), tile)
            upper, lower = two_parts(dot(src[rows, :], basis))
            dims = (((0,), (0,)), ((), ()))
            cots = cot[rows, :]
            acc[...] += dot(upper, cots, dims) + dot(lower, cots, dims)
            return carry
        lax.fori_loop(0, tokens // tile, body, 0)

    project(mo_ref, oc_ref, o_basis, oacc)
    project(x_ref, vc_ref, v_basis, vacc)
    r = vpart.shape[1]
    for i in range(n):
        vpart[i] = vacc[i * r:(i + 1) * r, :]
        opart[i] = oacc[i * r:(i + 1) * r, :]

    scatters = [
        Scatter(me, vpart, vrs, vstage, order_a[::-1], s_send.at[0], s_recv.at[0]),
        Scatter(me, opart, ors, ostage, order_b[::-1], s_send.at[1], s_recv.at[1]),
    ]
    for steps in zip(*[s.tasks() for s in scatters]):
        for s, js in zip(scatters, steps):
            s.run(js)

    def moments(projected, first, second, first_new, second_new):
        fn = first_decay * first[...] + (1.0 - first_decay) * projected
        sn = second_decay * second[...] + (1.0 - second_decay) * projected * projected
        first_new[...] = fn
        second_new[...] = sn
        return fn / jnp.sqrt(sn)

    zero = (0,) * len(digits)
    vdir[me] = moments(scatters[0].summed(zero), vf, vs, vf_new, vs_new)
    odir[me] = moments(scatters[1].summed(zero), of, os_, of_new, os_new)
    for s in scatters:
        s.drain()

    gather_all([
        Gather(me, vdir, order_a, g_send.at[2], g_recv.at[2]),
        Gather(me, odir, order_b, g_send.at[3], g_recv.at[3]),
    ])
    v_dir = merged(vdir)
    o_dir = merged(odir)
    squares[0] = jnp.full(squares.shape[1:], jnp.sum(v_dir * v_dir) + jnp.sum(o_dir * o_dir), jnp.float32)
    traded = []
    for off in range(1, m):
        c = pltpu.make_async_remote_copy(
            src_ref=squares.at[0], dst_ref=squares.at[off],
            send_sem=q_send.at[off], recv_sem=q_recv.at[off],
            device_id={"tp": lax.rem(mine + off, m)}, device_id_type=pl.DeviceIdType.MESH,
        )
        c.start()
        traded.append(c)
    v_upper, v_lower = two_parts(v_dir)
    o_upper, o_lower = two_parts(o_dir)
    v_sum = dot(vb[...], v_upper) + dot(vb[...], v_lower)
    o_sum = dot(ob[...], o_upper) + dot(ob[...], o_lower)
    for c in traded:
        c.wait()
    total = squares[0]
    for off in range(1, m):
        total = total + squares[off]
    scale = (step_rate / jnp.sqrt(1.0 + total / total_size))[0:1, 0:1]

    def update(weight, product, new, step, copy):
        s = scale * product
        w = weight[...] - s
        step[...] = s
        new[...] = w
        copy[me] = w.astype(jnp.bfloat16)

    update(vw, v_sum, vnew, vstep, vcopy)
    update(ow, o_sum, onew, ostep, ocopy)

    gather_all([
        Gather(me, vcopy, order_a, g_send.at[4], g_recv.at[4]),
        Gather(me, ocopy, order_b, g_send.at[5], g_recv.at[5]),
    ])


def local(n, m, x, vc, mo, oc, vw, ow, vb, ob, vf, vs, of, os_):
    f32, bf16 = jnp.float32, jnp.bfloat16
    shape = jax.ShapeDtypeStruct
    r, v_cols = vf.shape
    o_cols = of.shape[1]
    total_size = float(n * r * m * (v_cols + o_cols))
    vmem = pl.BlockSpec(memory_space=pltpu.VMEM)
    hbm = pl.BlockSpec(memory_space=pl.ANY)
    outs = (
        shape(vw.shape, f32), shape(ow.shape, f32),
        shape(vw.shape, f32), shape(ow.shape, f32),
        shape((n, *vw.shape), bf16), shape((n, *ow.shape), bf16),
        shape(vf.shape, f32), shape(vf.shape, f32), shape(of.shape, f32), shape(of.shape, f32),
    )
    dma = pltpu.SemaphoreType.DMA
    res = pl.pallas_call(
        functools.partial(kernel, n, m, total_size),
        out_shape=outs,
        in_specs=[hbm] * 4 + [vmem] * 8,
        out_specs=[vmem] * 10,
        scratch_shapes=[
            pltpu.VMEM(x.shape, bf16), pltpu.VMEM(vc.shape, bf16),
            pltpu.VMEM(mo.shape, bf16), pltpu.VMEM(oc.shape, bf16),
            pltpu.VMEM((n, *vb.shape), bf16), pltpu.VMEM((n, *ob.shape), bf16),
            pltpu.VMEM((n, r, v_cols), f32), pltpu.VMEM((n, r, o_cols), f32),
            pltpu.VMEM((n * r, v_cols), f32), pltpu.VMEM((n * r, o_cols), f32),
            pltpu.VMEM((n, r, v_cols), f32), pltpu.VMEM((n, r, o_cols), f32),
            pltpu.VMEM((n, r, v_cols), f32), pltpu.VMEM((n, r, o_cols), f32),
            pltpu.VMEM((n, r, v_cols), f32), pltpu.VMEM((n, r, o_cols), f32),
            pltpu.VMEM((m, 8, 128), f32),
            dma((4,)), dma((6, n)), dma((6, n)), dma((2, n)), dma((2, n)), dma((m,)), dma((m,)),
        ],
        compiler_params=pltpu.CompilerParams(
            collective_id=0, has_side_effects=True, vmem_limit_bytes=60 * 1024 * 1024
        ),
    )(x, vc, mo, oc, vw, ow, vb, ob, vf, vs, of, os_)
    vcopy, ocopy = res[4], res[5]
    return (
        *res[:4],
        vcopy.reshape(n * vw.shape[0], v_cols),
        ocopy.reshape(n * ow.shape[0], o_cols),
        *res[6:],
    )


def solution(mesh):
    n, m = mesh.shape["fs"], mesh.shape["tp"]
    rows, both, cols = P("fs", None), P("fs", "tp"), P(None, "tp")
    return jax.shard_map(
        functools.partial(local, n, m),
        mesh=mesh,
        in_specs=(rows, both, rows, both, both, both, rows, rows, both, both, both, both),
        out_specs=(both, both, both, both, cols, cols, both, both, both, both),
        check_vma=False,
    )
```

time: 421 us -> 141 us (0.33)
  the two profiles are of different devices: /device:TPU:0 before, /device:TPU:16 now
where the time goes in v1:
time: 141 us
  Pallas kernels  127 us (90%)
  local copies, waits for them, and re-layouts  13 us (9%)
    pallas_call x1, Pallas kernels, local(): pl.pallas_call(functools.partial(kernel, n, m, total_size), out_shape=out...  127 us
    unnamed x22, local copies, waits for them, and re-layouts  13 us

profile of v1, /device:TPU:16, one launch (start us, length us, event | category | flops | bytes accessed | tf_op | source)
XLA Modules:
  0.0 141.0 jit_solution(18184151853704914541)
XLA Ops:
  0.6 127.3 %shard_map.195 = (f32[128,512]{1,0:T(8,128)}, f32[64,1024]{1,0:T(8,128)}, f32[128,512]{1,0:T(8,128)}, f32[64,1024]{1,0:T(8,128)}, bf16[16,128,512]{2,1,0:T(8,128...) custom-call(bf16[1024,2048]{1,0:T(8,128)(2,1)} %x_hbm.1, ...), custom_call_target="tpu_custom_call" | custom-call | tf_op jit(solution)/shard_map/pallas_call | solution.py:330
  128.0 0.0 copy-start.1
  128.0 1.8 %copy.32 = f32[128,512]{1,0:T(8,128)} copy(f32[128,512]{1,0:T(8,128)} %get-tuple-element.40) | data formatting | bytes 524288
  129.8 1.7 %copy.33 = f32[64,1024]{1,0:T(8,128)} copy(f32[64,1024]{1,0:T(8,128)} %get-tuple-element.41) | data formatting | bytes 524288
  131.5 1.7 %copy.34 = f32[128,512]{1,0:T(8,128)} copy(f32[128,512]{1,0:T(8,128)} %get-tuple-element.42) | data formatting | bytes 524288
  133.1 1.7 %copy.35 = f32[64,1024]{1,0:T(8,128)} copy(f32[64,1024]{1,0:T(8,128)} %get-tuple-element.43) | data formatting | bytes 524288
  134.8 0.0 copy-done.1
  134.8 0.0 copy-start
  134.8 1.3 copy.36
  136.1 1.0 copy-done
  137.2 0.0 copy-start.5
  137.2 0.0 copy-start.4
  137.2 0.0 copy-start.3
  137.2 0.0 copy-start.2
  137.2 1.3 copy.37
  138.5 0.0 copy-done.5
  138.5 0.6 copy.38
  139.1 0.0 copy-done.4
  139.1 0.6 copy.39
  139.7 0.0 copy-done.3
  139.7 0.6 copy.40
  140.4 0.0 copy-done.2
  140.4 0.6 copy.41
Async XLA Ops:
  128.0 6.8 %copy-start.1 = (bf16[16,128,512]{2,1,0:T(8,128)(2,1)S(1)}, bf16[16,128,512]{2,1,0:T(8,128)(2,1)}, u32[]{:S(2)}) copy-start(bf16[16,128,512]{2,1,0:T(8,128)(2,1)} %get-tuple-element.24) | copy-start | bytes 6291460
  134.8 2.3 %copy-start = (bf16[16,64,1024]{2,1,0:T(8,128)(2,1)S(1)}, bf16[16,64,1024]{2,1,0:T(8,128)(2,1)}, u32[]{:S(2)}) copy-start(bf16[16,64,1024]{2,1,0:T(8,128)(2,1)} %get-tuple-element.25) | copy-start | bytes 6291460
  137.2 1.3 copy-start.5
  137.2 2.0 %copy-start.4 = (f32[16,512]{1,0:T(8,128)S(1)}, f32[16,512]{1,0:T(8,128)}, u32[]{:S(2)}) copy-start(f32[16,512]{1,0:T(8,128)} %get-tuple-element.47) | copy-start | bytes 98308
  137.2 2.6 %copy-start.3 = (f32[16,1024]{1,0:T(8,128)S(1)}, f32[16,1024]{1,0:T(8,128)}, u32[]{:S(2)}) copy-start(f32[16,1024]{1,0:T(8,128)} %get-tuple-element.48) | copy-start | bytes 196612
  137.2 3.2 %copy-start.2 = (f32[16,1024]{1,0:T(8,128)S(1)}, f32[16,1024]{1,0:T(8,128)}, u32[]{:S(2)}) copy-start(f32[16,1024]{1,0:T(8,128)} %get-tuple-element.49) | copy-start | bytes 196612

commit v2 on v1

--- a/solution.py
+++ b/solution.py
@@ -47,62 +47,111 @@
     return out
 
 
+class Line:
+    def __init__(self, me, digit):
+        self.size, self.stride = digit
+        self.me = me
+        self.at = lax.div(me, self.stride)
+
+    def nearest(self, t):
+        if t == 0:
+            return self.at
+        k, z = self.size, self.at
+        near = jnp.minimum(z, k - 1 - z)
+        low = z < k - 1 - z
+        step = (t + 1) // 2 if t % 2 else -(t // 2)
+        both = jnp.where(low, z - step, z + step)
+        one = jnp.where(low, z + (t - near), z - (t - near))
+        return jnp.where(t <= 2 * near, both, one)
+
+
 class Gather:
     def __init__(self, me, dst, order, send_sem, recv_sem):
         self.me, self.dst, self.order = me, dst, order
+        self.line = Line(me, order[0])
         self.send_sem, self.recv_sem = send_sem, recv_sem
         self.sent = []
 
-    def copy(self, held, axis, off):
-        target = tuple(off if i == axis else h for i, h in enumerate(held))
-        slot = flat(self.order, target)
-        block = shifted(self.me, self.order, held, -1)
-        peer = shifted(self.me, self.order, tuple(off if i == axis else 0 for i in range(len(held))), 1)
+    def events(self):
+        fast = list(itertools.product(*[range(s) for s, _ in self.order[1:]]))
+        rows = []
+        for t in range(self.order[0][0]):
+            for js in fast:
+                phase = max([i + 1 for i, j in enumerate(js) if j], default=0)
+                due = t + 1.25 * phase if phase < len(self.order) - 1 else 100 + t
+                rows.append((due, phase, t, js))
+        return sorted(rows)
+
+    def block(self, event):
+        _, _, t, js = event
+        z = self.line.nearest(t)
+        return shifted(self.me, self.order[1:], js, -1) + (z - self.line.at) * self.line.stride
+
+    def copy(self, block, peer, way):
         return pltpu.make_async_remote_copy(
-            src_ref=self.dst.at[block],
-            dst_ref=self.dst.at[block],
-            send_sem=self.send_sem.at[slot],
-            recv_sem=self.recv_sem.at[slot],
+            src_ref=self.dst(block),
+            dst_ref=self.dst(block),
+            send_sem=self.send_sem.at[block, way],
+            recv_sem=self.recv_sem.at[block],
             device_id={"fs": peer},
             device_id_type=pl.DeviceIdType.MESH,
         )
 
-    def forward(self, held):
-        last = max([i for i, h in enumerate(held) if h], default=-1)
-        for axis in range(last + 1, len(self.order)):
-            for off in range(1, self.order[axis][0]):
-                c = self.copy(held, axis, off)
-                c.start()
-                self.sent.append(c)
-
-    def arrive(self, held):
-        if any(held):
-            slot = flat(self.order, held)
-            block = shifted(self.me, self.order, held, -1)
-            pltpu.make_async_remote_copy(
-                src_ref=self.dst.at[block],
-                dst_ref=self.dst.at[block],
-                send_sem=self.send_sem.at[slot],
-                recv_sem=self.recv_sem.at[slot],
-                device_id={"fs": self.me},
-                device_id_type=pl.DeviceIdType.MESH,
-            ).wait_recv()
-
-    def all_held(self):
-        rows = list(itertools.product(*[range(s) for s, _ in self.order]))
-        return sorted(rows, key=lambda h: max([i for i, v in enumerate(h) if v], default=-1))
+    def start(self, cond, c):
+        if cond is None:
+            c.start()
+        else:
+            pl.when(cond)(c.start)
+        self.sent.append((cond, c))
+
+    def forward(self, event):
+        _, phase, t, js = event
+        block = self.block(event)
+        if phase == 0:
+            z, k, stride = self.line.at, self.line.size, self.line.stride
+            source = self.line.nearest(t)
+            up = z + 1 < k
+            down = z > 0
+            if t > 0:
+                up = jnp.logical_and(up, source < z)
+                down = jnp.logical_and(down, source > z)
+            self.start(up, self.copy(block, jnp.minimum(self.me + stride, k * stride - stride + lax.rem(self.me, stride)), 0))
+            self.start(down, self.copy(block, jnp.maximum(self.me - stride, lax.rem(self.me, stride)), 1))
+        way = 2
+        for axis in range(1, len(self.order)):
+            size = self.order[axis][0]
+            for off in range(1, size):
+                if axis > phase:
+                    peer = shifted(self.me, [self.order[axis]], (off,), 1)
+                    self.start(None, self.copy(block, peer, way))
+                way += 1
+
+    def arrive(self, event):
+        if event[2] or any(event[3]):
+            self.copy(self.block(event), shifted(self.me, [self.order[-1]], (1,), 1), 0).wait_recv()
 
     def drain(self):
-        for c in self.sent:
-            c.wait_send()
-
-
-def gather_all(gathers, started=()):
-    for steps in itertools.zip_longest(*[g.all_held() for g in gathers]):
-        for g, held in zip(gathers, steps):
-            if held is not None:
-                g.arrive(held)
-                g.forward(held)
+        for cond, c in self.sent:
+            if cond is None:
+                c.wait_send()
+            else:
+                pl.when(cond)(c.wait_send)
+
+
+def own_event(gather):
+    return gather.events()[0]
+
+
+def gather_all(gathers, then=None):
+    for g in gathers:
+        if not g.sent:
+            g.forward(own_event(g))
+    for steps in zip(*[g.events()[1:] for g in gathers]):
+        for i, (g, event) in enumerate(zip(gathers, steps)):
+            g.arrive(event)
+            g.forward(event)
+            if then is not None:
+                then(i, g.block(event))
     for g in gathers:
         g.drain()
 
@@ -177,28 +226,31 @@
     return jnp.concatenate([ref[i] for i in range(n)], axis=0)
 
 
+def merged_halves(ref):
+    n, h, r, c = ref.shape
+    if r % 16 == 0:
+        return ref[...].reshape(n * h * r, c)
+    return jnp.concatenate([ref[i, j] for i in range(n) for j in range(h)], axis=0)
+
+
 def kernel(
     n, m, total_size,
-    x_hbm, vc_hbm, mo_hbm, oc_hbm,
-    vw, ow, vb, ob, vf, vs, of, os_,
+    x_hbm, vc_hbm, mo_hbm, oc_hbm, vw_hbm, ow_hbm, vf_hbm, vs_hbm, of_hbm, os_hbm, vb, ob,
     vnew, onew, vstep, ostep, vcopy, ocopy, vf_new, vs_new, of_new, os_new,
-    x_ref, vc_ref, mo_ref, oc_ref,
+    x_ref, vc_ref, mo_ref, oc_ref, vw, ow, vf, vs, of, os_,
     vb_all, ob_all, vpart, opart, vacc, oacc, vrs, ors, vstage, ostage, vdir, odir, squares,
-    load_sem, g_send, g_recv, s_send, s_recv, q_send, q_recv,
+    load_sem, g_send, g_recv, s_send, s_recv, q_send, q_recv, p_send, p_recv,
 ):
     me = lax.axis_index("fs")
     mine = lax.axis_index("tp")
     digits = split_digits(n)
     order_a, order_b = orders_of(digits)
 
-    loads = [
-        pltpu.make_async_copy(src, dst, load_sem.at[i])
-        for i, (src, dst) in enumerate(((x_hbm, x_ref), (vc_hbm, vc_ref), (mo_hbm, mo_ref), (oc_hbm, oc_ref)))
-    ]
-    for c in loads:
-        c.start()
-    vb_all[me] = vb[...]
-    ob_all[me] = ob[...]
+    pairs = (
+        (mo_hbm, mo_ref), (oc_hbm, oc_ref), (x_hbm, x_ref), (vc_hbm, vc_ref),
+        (vf_hbm, vf), (vs_hbm, vs), (of_hbm, of), (os_hbm, os_), (vw_hbm, vw), (ow_hbm, ow),
+    )
+    loads = [pltpu.make_async_copy(src, dst, load_sem.at[i]) for i, (src, dst) in enumerate(pairs)]
 
     barrier = pltpu.get_barrier_semaphore()
     peers = 0
@@ -215,23 +267,49 @@
             device_id_type=pl.DeviceIdType.MESH,
         )
         peers += 1
+    for c in loads:
+        c.start()
+    halves = vb_all.shape[1]
+    for whole, held in ((vb, vb_all), (ob, ob_all)):
+        rows = held.shape[2]
+        for h in range(halves):
+            held[me, h] = whole[h * rows:(h + 1) * rows, :]
     pl.semaphore_wait(barrier, peers)
 
+    half = lax.rem(mine, halves)
+    sibling = mine + 1 - 2 * half
+    bases = (vb_all, ob_all)
+
+    def hand(i, block, part):
+        return pltpu.make_async_remote_copy(
+            src_ref=bases[i].at[block, part], dst_ref=bases[i].at[block, part],
+            send_sem=p_send.at[i, block], recv_sem=p_recv.at[i, block],
+            device_id={"tp": sibling}, device_id_type=pl.DeviceIdType.MESH,
+        )
+
+    handed = []
+
+    def share(i, block):
+        if halves == 2:
+            c = hand(i, block, half)
+            c.start()
+            handed.append((i, block, c))
+
     gather_all([
-        Gather(me, vb_all, order_a, g_send.at[0], g_recv.at[0]),
-        Gather(me, ob_all, order_b, g_send.at[1], g_recv.at[1]),
-    ])
-    for c in loads:
-        c.wait()
+        Gather(me, lambda b: vb_all.at[b, half], order_a, g_send.at[0], g_recv.at[0]),
+        Gather(me, lambda b: ob_all.at[b, half], order_b, g_send.at[1], g_recv.at[1]),
+    ], share)
+    for i, block, c in handed:
+        c.wait_send()
+        hand(i, block, 1 - half).wait_recv()
 
     tokens = x_ref.shape[0]
     tile = min(256, tokens)
-    v_basis = merged(vb_all)
-    o_basis = merged(ob_all)
-    vacc[...] = jnp.zeros_like(vacc)
-    oacc[...] = jnp.zeros_like(oacc)
-
-    def project(src, cot, basis, acc):
+    r = vpart.shape[1]
+
+    def project(src, cot, basis, acc, part):
+        acc[...] = jnp.zeros_like(acc)
+
         def body(t, carry):
             rows = pl.ds(pl.multiple_of(t * tile, tile), tile)
             upper, lower = two_parts(dot(src[rows, :], basis))
@@ -240,21 +318,29 @@
             acc[...] += dot(upper, cots, dims) + dot(lower, cots, dims)
             return carry
         lax.fori_loop(0, tokens // tile, body, 0)
-
-    project(mo_ref, oc_ref, o_basis, oacc)
-    project(x_ref, vc_ref, v_basis, vacc)
-    r = vpart.shape[1]
-    for i in range(n):
-        vpart[i] = vacc[i * r:(i + 1) * r, :]
-        opart[i] = oacc[i * r:(i + 1) * r, :]
-
-    scatters = [
-        Scatter(me, vpart, vrs, vstage, order_a[::-1], s_send.at[0], s_recv.at[0]),
-        Scatter(me, opart, ors, ostage, order_b[::-1], s_send.at[1], s_recv.at[1]),
-    ]
-    for steps in zip(*[s.tasks() for s in scatters]):
-        for s, js in zip(scatters, steps):
-            s.run(js)
+        for i in range(n):
+            part[i] = acc[i * r:(i + 1) * r, :]
+
+    scatter_v = Scatter(me, vpart, vrs, vstage, order_a[::-1], s_send.at[0], s_recv.at[0])
+    scatter_o = Scatter(me, opart, ors, ostage, order_b[::-1], s_send.at[1], s_recv.at[1])
+    loads[0].wait()
+    loads[1].wait()
+    project(mo_ref, oc_ref, merged_halves(ob_all), oacc, opart)
+    tasks_o = scatter_o.tasks()
+    early = [js for js in tasks_o if js[0]]
+    for js in early:
+        scatter_o.run(js)
+    loads[2].wait()
+    loads[3].wait()
+    project(x_ref, vc_ref, merged_halves(vb_all), vacc, vpart)
+    tasks_v = scatter_v.tasks()
+    for js in tasks_v[:len(early)]:
+        scatter_v.run(js)
+    for js_o, js_v in zip(tasks_o[len(early):], tasks_v[len(early):]):
+        scatter_o.run(js_o)
+        scatter_v.run(js_v)
+    for c in loads[4:]:
+        c.wait()
 
     def moments(projected, first, second, first_new, second_new):
         fn = first_decay * first[...] + (1.0 - first_decay) * projected
@@ -264,15 +350,17 @@
         return fn / jnp.sqrt(sn)
 
     zero = (0,) * len(digits)
-    vdir[me] = moments(scatters[0].summed(zero), vf, vs, vf_new, vs_new)
-    odir[me] = moments(scatters[1].summed(zero), of, os_, of_new, os_new)
-    for s in scatters:
-        s.drain()
-
-    gather_all([
-        Gather(me, vdir, order_a, g_send.at[2], g_recv.at[2]),
-        Gather(me, odir, order_b, g_send.at[3], g_recv.at[3]),
-    ])
+    gathers = [
+        Gather(me, lambda b: odir.at[b], order_b, g_send.at[1], g_recv.at[3]),
+        Gather(me, lambda b: vdir.at[b], order_a, g_send.at[0], g_recv.at[2]),
+    ]
+    odir[me] = moments(scatter_o.summed(zero), of, os_, of_new, os_new)
+    gathers[0].forward(own_event(gathers[0]))
+    vdir[me] = moments(scatter_v.summed(zero), vf, vs, vf_new, vs_new)
+    gathers[1].forward(own_event(gathers[1]))
+    scatter_o.drain()
+    scatter_v.drain()
+    gather_all(gathers)
     v_dir = merged(vdir)
     o_dir = merged(odir)
     squares[0] = jnp.full(squares.shape[1:], jnp.sum(v_dir * v_dir) + jnp.sum(o_dir * o_dir), jnp.float32)
@@ -303,51 +391,73 @@
         new[...] = w
         copy[me] = w.astype(jnp.bfloat16)
 
+    gathers = [
+        Gather(me, lambda b: vcopy.at[b], order_a, g_send.at[0], g_recv.at[4]),
+        Gather(me, lambda b: ocopy.at[b], order_b, g_send.at[1], g_recv.at[5]),
+    ]
     update(vw, v_sum, vnew, vstep, vcopy)
+    gathers[0].forward(own_event(gathers[0]))
     update(ow, o_sum, onew, ostep, ocopy)
-
-    gather_all([
-        Gather(me, vcopy, order_a, g_send.at[4], g_recv.at[4]),
-        Gather(me, ocopy, order_b, g_send.at[5], g_recv.at[5]),
-    ])
+    gather_all(gathers)
+
+
+def store(*refs):
+    count = (len(refs) - 1) // 2
+    ins, outs, sems = refs[:count], refs[count:2 * count], refs[-1]
+    copies = [pltpu.make_async_copy(i, o, sems.at[k]) for k, (i, o) in enumerate(zip(ins, outs))]
+    for c in copies:
+        c.start()
+    for c in copies:
+        c.wait()
 
 
 def local(n, m, x, vc, mo, oc, vw, ow, vb, ob, vf, vs, of, os_):
     f32, bf16 = jnp.float32, jnp.bfloat16
-    shape = jax.ShapeDtypeStruct
     r, v_cols = vf.shape
     o_cols = of.shape[1]
     total_size = float(n * r * m * (v_cols + o_cols))
+    halves = 2 if m % 2 == 0 else 1
     vmem = pl.BlockSpec(memory_space=pltpu.VMEM)
-    hbm = pl.BlockSpec(memory_space=pl.ANY)
+    hbm = pl.BlockSpec(memory_space=pltpu.HBM)
+    anywhere = pl.BlockSpec(memory_space=pl.ANY)
     outs = (
-        shape(vw.shape, f32), shape(ow.shape, f32),
-        shape(vw.shape, f32), shape(ow.shape, f32),
-        shape((n, *vw.shape), bf16), shape((n, *ow.shape), bf16),
-        shape(vf.shape, f32), shape(vf.shape, f32), shape(of.shape, f32), shape(of.shape, f32),
+        (vw.shape, f32), (ow.shape, f32), (vw.shape, f32), (ow.shape, f32),
+        ((n, *vw.shape), bf16), ((n, *ow.shape), bf16),
+        (vf.shape, f32), (vf.shape, f32), (of.shape, f32), (of.shape, f32),
     )
     dma = pltpu.SemaphoreType.DMA
+    big = (x, vc, mo, oc, vw, ow, vf, vs, of, os_)
+    ways = 2 + sum(s - 1 for s, _ in split_digits(n)[:-1])
     res = pl.pallas_call(
         functools.partial(kernel, n, m, total_size),
-        out_shape=outs,
-        in_specs=[hbm] * 4 + [vmem] * 8,
+        out_shape=tuple(pltpu.VMEM(s, d) for s, d in outs),
+        in_specs=[hbm] * 10 + [vmem] * 2,
         out_specs=[vmem] * 10,
         scratch_shapes=[
-            pltpu.VMEM(x.shape, bf16), pltpu.VMEM(vc.shape, bf16),
-            pltpu.VMEM(mo.shape, bf16), pltpu.VMEM(oc.shape, bf16),
-            pltpu.VMEM((n, *vb.shape), bf16), pltpu.VMEM((n, *ob.shape), bf16),
+            *[pltpu.VMEM(a.shape, a.dtype) for a in big],
+            pltpu.VMEM((n, halves, vb.shape[0] // halves, vb.shape[1]), bf16),
+            pltpu.VMEM((n, halves, ob.shape[0] // halves, ob.shape[1]), bf16),
             pltpu.VMEM((n, r, v_cols), f32), pltpu.VMEM((n, r, o_cols), f32),
             pltpu.VMEM((n * r, v_cols), f32), pltpu.VMEM((n * r, o_cols), f32),
             pltpu.VMEM((n, r, v_cols), f32), pltpu.VMEM((n, r, o_cols), f32),
             pltpu.VMEM((n, r, v_cols), f32), pltpu.VMEM((n, r, o_cols), f32),
             pltpu.VMEM((n, r, v_cols), f32), pltpu.VMEM((n, r, o_cols), f32),
             pltpu.VMEM((m, 8, 128), f32),
-            dma((4,)), dma((6, n)), dma((6, n)), dma((2, n)), dma((2, n)), dma((m,)), dma((m,)),
+            dma((10,)), dma((2, n, ways)), dma((6, n)), dma((2, n)), dma((2, n)), dma((m,)), dma((m,)),
+            dma((2, n)), dma((2, n)),
         ],
         compiler_params=pltpu.CompilerParams(
-            collective_id=0, has_side_effects=True, vmem_limit_bytes=60 * 1024 * 1024
+            collective_id=0, has_side_effects=True, vmem_limit_bytes=36 * 1024 * 1024
         ),
-    )(x, vc, mo, oc, vw, ow, vb, ob, vf, vs, of, os_)
+    )(*[pltpu.with_memory_space_constraint(a, pltpu.HBM) for a in big], vb, ob)
+    res = pl.pallas_call(
+        store,
+        out_shape=tuple(jax.ShapeDtypeStruct(s, d) for s, d in outs),
+        in_specs=[anywhere] * 10,
+        out_specs=[hbm] * 10,
+        scratch_shapes=[dma((10,))],
+        compiler_params=pltpu.CompilerParams(vmem_limit_bytes=1024 * 1024),
+    )(*res)
     vcopy, ocopy = res[4], res[5]
     return (
         *res[:4],

time: 141 us -> 110 us (0.78)
  the two profiles are of different devices: /device:TPU:16 before, /device:TPU:0 now
where the time goes in v2:
time: 110 us
  Pallas kernels  108 us (98%)
  local copies, waits for them, and re-layouts  1.59 us (1%)
    pallas_call x1, Pallas kernels, local(): pl.pallas_call(functools.partial(kernel, n, m, total_size), out_shape=tup...  106 us
    pallas_call x1, Pallas kernels, local(): pl.pallas_call(store, out_shape=tuple((jax.ShapeDtypeStruct(s, d) for s,...  2.49 us

profile of v2, /device:TPU:0, one launch (start us, length us, event | category | flops | bytes accessed | tf_op | source)
XLA Modules:
  0.0 110.3 jit_solution(4391030390914847006)
XLA Ops:
  0.6 0.0 copy-start
  0.7 0.8 copy-done
  1.5 0.0 copy-start.1
  1.5 0.8 copy-done.1
  2.2 105.5 %shard_map.195 = (f32[128,512]{1,0:T(8,128)S(1)}, f32[64,1024]{1,0:T(8,128)S(1)}, f32[128,512]{1,0:T(8,128)S(1)}, f32[64,1024]{1,0:T(8,128)S(1)}, bf16[16,128,51...) custom-call(bf16[1024,2048]{1,0:T(8,128)(2,1)} %x_hbm.1, ...), custom_call_target="tpu_custom_call" | custom-call | tf_op jit(solution)/shard_map/pallas_call | solution.py:431
  107.8 2.5 %shard_map.196 = (f32[128,512]{1,0:T(8,128)}, f32[64,1024]{1,0:T(8,128)}, f32[128,512]{1,0:T(8,128)}, f32[64,1024]{1,0:T(8,128)}, bf16[16,128,512]{2,1,0:T(8,128...) custom-call(f32[128,512]{1,0:T(8,128)S(1)} %get-tuple-element.30.ref, ...), custom_call_target="tpu_custom_call" | custom-call | tf_op jit(solution)/shard_map/pallas_call | solution.py:453
Async XLA Ops:
  0.6 0.8 copy-start
  1.5 0.8 copy-start.1

commit v3 on v2

--- a/solution.py
+++ b/solution.py
@@ -27,7 +27,8 @@
 
 def orders_of(digits):
     slow, fast = digits[-1], digits[:-1]
-    return [slow, *fast], [slow, *fast[::-1]]
+    back = fast[::-1]
+    return [slow, *fast], [slow, *back], [fast[0], slow, *fast[1:]], [back[0], slow, *back[1:]]
 
 
 def shifted(me, order, offsets, sign):
@@ -66,32 +67,36 @@
 
 
 class Gather:
-    def __init__(self, me, dst, order, send_sem, recv_sem):
+    def __init__(self, me, dst, order, slow, send_sem, recv_sem, line_sem=None):
         self.me, self.dst, self.order = me, dst, order
-        self.line = Line(me, order[0])
-        self.send_sem, self.recv_sem = send_sem, recv_sem
+        self.slow = order.index(slow)
+        self.line = Line(me, slow)
+        self.send_sem, self.recv_sem, self.line_sem = send_sem, recv_sem, line_sem
         self.sent = []
 
     def events(self):
-        fast = list(itertools.product(*[range(s) for s, _ in self.order[1:]]))
         rows = []
-        for t in range(self.order[0][0]):
-            for js in fast:
-                phase = max([i + 1 for i, j in enumerate(js) if j], default=0)
-                due = t + 1.25 * phase if phase < len(self.order) - 1 else 100 + t
-                rows.append((due, phase, t, js))
+        last = len(self.order) - 1
+        for at in itertools.product(*[range(s) for s, _ in self.order]):
+            phase = max([i for i, j in enumerate(at) if j], default=-1)
+            due = sum(j if i == self.slow else 1.25 * (j > 0) for i, j in enumerate(at))
+            if phase == last and last != self.slow:
+                due += 100
+            rows.append((due, phase, at))
         return sorted(rows)
 
     def block(self, event):
-        _, _, t, js = event
-        z = self.line.nearest(t)
-        return shifted(self.me, self.order[1:], js, -1) + (z - self.line.at) * self.line.stride
-
-    def copy(self, block, peer, way):
+        at = event[2]
+        fast = [d for i, d in enumerate(self.order) if i != self.slow]
+        offs = [j for i, j in enumerate(at) if i != self.slow]
+        z = self.line.nearest(at[self.slow])
+        return shifted(self.me, fast, offs, -1) + (z - self.line.at) * self.line.stride
+
+    def copy(self, block, peer, send):
         return pltpu.make_async_remote_copy(
             src_ref=self.dst(block),
             dst_ref=self.dst(block),
-            send_sem=self.send_sem.at[block, way],
+            send_sem=send,
             recv_sem=self.recv_sem.at[block],
             device_id={"fs": peer},
             device_id_type=pl.DeviceIdType.MESH,
@@ -104,31 +109,44 @@
             pl.when(cond)(c.start)
         self.sent.append((cond, c))
 
+    def along_line(self, block, t):
+        z, k, stride = self.line.at, self.line.size, self.line.stride
+        if self.line_sem is not None:
+            if t == 0:
+                for other in range(1, k):
+                    peer = self.me + (self.line.nearest(other) - z) * stride
+                    self.start(None, self.copy(block, peer, self.line_sem.at[other]))
+            return
+        up = z + 1 < k
+        down = z > 0
+        if t > 0:
+            source = self.line.nearest(t)
+            up = jnp.logical_and(up, source < z)
+            down = jnp.logical_and(down, source > z)
+        base = lax.rem(self.me, stride)
+        self.start(up, self.copy(block, jnp.minimum(self.me + stride, (k - 1) * stride + base), self.send_sem.at[block, 0]))
+        self.start(down, self.copy(block, jnp.maximum(self.me - stride, base), self.send_sem.at[block, 1]))
+
     def forward(self, event):
-        _, phase, t, js = event
+        _, phase, at = event
         block = self.block(event)
-        if phase == 0:
-            z, k, stride = self.line.at, self.line.size, self.line.stride
-            source = self.line.nearest(t)
-            up = z + 1 < k
-            down = z > 0
-            if t > 0:
-                up = jnp.logical_and(up, source < z)
-                down = jnp.logical_and(down, source > z)
-            self.start(up, self.copy(block, jnp.minimum(self.me + stride, k * stride - stride + lax.rem(self.me, stride)), 0))
-            self.start(down, self.copy(block, jnp.maximum(self.me - stride, lax.rem(self.me, stride)), 1))
         way = 2
-        for axis in range(1, len(self.order)):
-            size = self.order[axis][0]
-            for off in range(1, size):
+        for axis, digit in enumerate(self.order):
+            if axis == self.slow:
+                if axis >= phase:
+                    self.along_line(block, at[axis])
+                continue
+            for off in range(1, digit[0]):
                 if axis > phase:
-                    peer = shifted(self.me, [self.order[axis]], (off,), 1)
-                    self.start(None, self.copy(block, peer, way))
+                    peer = shifted(self.me, [digit], (off,), 1)
+                    self.start(None, self.copy(block, peer, self.send_sem.at[block, way]))
                 way += 1
 
     def arrive(self, event):
-        if event[2] or any(event[3]):
-            self.copy(self.block(event), shifted(self.me, [self.order[-1]], (1,), 1), 0).wait_recv()
+        if any(event[2]):
+            block = self.block(event)
+            fast = self.order[0 if self.slow else 1]
+            self.copy(block, shifted(self.me, [fast], (1,), 1), self.send_sem.at[block, 0]).wait_recv()
 
     def drain(self):
         for cond, c in self.sent:
@@ -157,8 +175,8 @@
 
 
 class Scatter:
-    def __init__(self, me, part, bufs, stage, order, send_sem, recv_sem):
-        self.me, self.part, self.bufs, self.stage = me, part, bufs, stage
+    def __init__(self, me, part, bufs, stage, cut, order, send_sem, recv_sem):
+        self.me, self.part, self.bufs, self.stage, self.cut = me, part, bufs, stage, cut
         self.order, self.send_sem, self.recv_sem = order, send_sem, recv_sem
         self.sent = []
 
@@ -169,10 +187,10 @@
         axis = next(i for i, j in enumerate(js) if j)
         slot = self.slot(js)
         peer = shifted(self.me, self.order, tuple(j if i == axis else 0 for i, j in enumerate(js)), 1)
-        src = self.part.at[shifted(self.me, self.order, js, 1)] if axis == 0 else self.stage.at[slot]
+        src = self.part.at[shifted(self.me, self.order, js, 1), self.cut] if axis == 0 else self.stage.at[slot, self.cut]
         return pltpu.make_async_remote_copy(
             src_ref=src,
-            dst_ref=self.bufs.at[slot],
+            dst_ref=self.bufs.at[slot, self.cut],
             send_sem=self.send_sem.at[slot],
             recv_sem=self.recv_sem.at[slot],
             device_id={"fs": peer},
@@ -181,12 +199,12 @@
 
     def summed(self, js):
         axis = next((i for i, j in enumerate(js) if j), len(js))
-        total = self.part[shifted(self.me, self.order, js, 1)]
+        total = self.part[shifted(self.me, self.order, js, 1), self.cut]
         for i in range(axis):
             for off in range(1, self.order[i][0]):
                 src = tuple(off if k == i else (js[k] if k > i else 0) for k in range(len(js)))
                 self.copy(src).wait_recv()
-                total = total + self.bufs[self.slot(src)]
+                total = total + self.bufs[self.slot(src), self.cut]
         return total
 
     def tasks(self):
@@ -199,7 +217,7 @@
             return
         axis = next(i for i, j in enumerate(js) if j)
         if axis > 0:
-            self.stage[self.slot(js)] = self.summed(js)
+            self.stage[self.slot(js), self.cut] = self.summed(js)
         c = self.copy(js)
         c.start()
         self.sent.append(c)
@@ -220,33 +238,28 @@
 
 
 def merged(ref):
-    n, r, c = ref.shape
-    if r % 8 == 0:
-        return ref[...].reshape(n * r, c)
-    return jnp.concatenate([ref[i] for i in range(n)], axis=0)
-
-
-def merged_halves(ref):
     n, h, r, c = ref.shape
-    if r % 16 == 0:
+    if r % (32 // ref.dtype.itemsize) == 0:
         return ref[...].reshape(n * h * r, c)
     return jnp.concatenate([ref[i, j] for i in range(n) for j in range(h)], axis=0)
 
 
 def kernel(
     n, m, total_size,
-    x_hbm, vc_hbm, mo_hbm, oc_hbm, vw_hbm, ow_hbm, vf_hbm, vs_hbm, of_hbm, os_hbm, vb, ob,
+    x_hbm, vc_hbm, mo_hbm, oc_hbm, vw_hbm, ow_hbm, vf_hbm, vs_hbm, of_hbm, os_hbm, vb_hbm, ob_hbm,
     vnew, onew, vstep, ostep, vcopy, ocopy, vf_new, vs_new, of_new, os_new,
-    x_ref, vc_ref, mo_ref, oc_ref, vw, ow, vf, vs, of, os_,
+    x_ref, vc_ref, mo_ref, oc_ref, vw, ow, vf, vs, of, os_, vb, ob,
     vb_all, ob_all, vpart, opart, vacc, oacc, vrs, ors, vstage, ostage, vdir, odir, squares,
-    load_sem, g_send, g_recv, s_send, s_recv, q_send, q_recv, p_send, p_recv,
+    load_sem, g_send, g_recv, s_send, s_recv, q_send, q_recv, p_send, p_recv, z_send,
 ):
     me = lax.axis_index("fs")
     mine = lax.axis_index("tp")
     digits = split_digits(n)
-    order_a, order_b = orders_of(digits)
+    order_a, order_b, order_c, order_d = orders_of(digits)
+    slow = digits[-1]
 
     pairs = (
+        (vb_hbm, vb), (ob_hbm, ob),
         (mo_hbm, mo_ref), (oc_hbm, oc_ref), (x_hbm, x_ref), (vc_hbm, vc_ref),
         (vf_hbm, vf), (vs_hbm, vs), (of_hbm, of), (os_hbm, os_), (vw_hbm, vw), (ow_hbm, ow),
     )
@@ -270,6 +283,8 @@
     for c in loads:
         c.start()
     halves = vb_all.shape[1]
+    loads[0].wait()
+    loads[1].wait()
     for whole, held in ((vb, vb_all), (ob, ob_all)):
         rows = held.shape[2]
         for h in range(halves):
@@ -296,8 +311,8 @@
             handed.append((i, block, c))
 
     gather_all([
-        Gather(me, lambda b: vb_all.at[b, half], order_a, g_send.at[0], g_recv.at[0]),
-        Gather(me, lambda b: ob_all.at[b, half], order_b, g_send.at[1], g_recv.at[1]),
+        Gather(me, lambda b: vb_all.at[b, half], order_a, slow, g_send.at[0], g_recv.at[0], z_send.at[0]),
+        Gather(me, lambda b: ob_all.at[b, half], order_b, slow, g_send.at[1], g_recv.at[1], z_send.at[1]),
     ], share)
     for i, block, c in handed:
         c.wait_send()
@@ -305,7 +320,7 @@
 
     tokens = x_ref.shape[0]
     tile = min(256, tokens)
-    r = vpart.shape[1]
+    cuts, r = vpart.shape[1:3]
 
     def project(src, cot, basis, acc, part):
         acc[...] = jnp.zeros_like(acc)
@@ -319,48 +334,65 @@
             return carry
         lax.fori_loop(0, tokens // tile, body, 0)
         for i in range(n):
-            part[i] = acc[i * r:(i + 1) * r, :]
-
-    scatter_v = Scatter(me, vpart, vrs, vstage, order_a[::-1], s_send.at[0], s_recv.at[0])
-    scatter_o = Scatter(me, opart, ors, ostage, order_b[::-1], s_send.at[1], s_recv.at[1])
-    loads[0].wait()
-    loads[1].wait()
-    project(mo_ref, oc_ref, merged_halves(ob_all), oacc, opart)
-    tasks_o = scatter_o.tasks()
-    early = [js for js in tasks_o if js[0]]
-    for js in early:
-        scatter_o.run(js)
+            for h in range(cuts):
+                part[i, h] = acc[(i * cuts + h) * r:(i * cuts + h + 1) * r, :]
+
+    turns = ((order_a, order_b), (order_b, order_a))
+    scatters_v = [
+        Scatter(me, vpart, vrs, vstage, h, turns[0][h % 2][::-1], s_send.at[h], s_recv.at[h])
+        for h in range(cuts)
+    ]
+    scatters_o = [
+        Scatter(me, opart, ors, ostage, h, turns[1][h % 2][::-1], s_send.at[cuts + h], s_recv.at[cuts + h])
+        for h in range(cuts)
+    ]
     loads[2].wait()
     loads[3].wait()
-    project(x_ref, vc_ref, merged_halves(vb_all), vacc, vpart)
-    tasks_v = scatter_v.tasks()
-    for js in tasks_v[:len(early)]:
-        scatter_v.run(js)
-    for js_o, js_v in zip(tasks_o[len(early):], tasks_v[len(early):]):
-        scatter_o.run(js_o)
-        scatter_v.run(js_v)
-    for c in loads[4:]:
+    project(mo_ref, oc_ref, merged(ob_all), oacc, opart)
+    def run(scatters, first):
+        lists = [[js for js in sc.tasks() if bool(js[0]) == first] for sc in scatters]
+        for steps in zip(*lists):
+            for sc, js in zip(scatters, steps):
+                sc.run(js)
+
+    run(scatters_o, True)
+    loads[4].wait()
+    loads[5].wait()
+    project(x_ref, vc_ref, merged(vb_all), vacc, vpart)
+    run(scatters_v, True)
+    run(scatters_o + scatters_v, False)
+    for c in loads[6:]:
         c.wait()
 
-    def moments(projected, first, second, first_new, second_new):
-        fn = first_decay * first[...] + (1.0 - first_decay) * projected
-        sn = second_decay * second[...] + (1.0 - second_decay) * projected * projected
-        first_new[...] = fn
-        second_new[...] = sn
+    def moments(projected, h, first, second, first_new, second_new):
+        rows = slice(h * r, (h + 1) * r)
+        fn = first_decay * first[rows, :] + (1.0 - first_decay) * projected
+        sn = second_decay * second[rows, :] + (1.0 - second_decay) * projected * projected
+        first_new[rows, :] = fn
+        second_new[rows, :] = sn
         return fn / jnp.sqrt(sn)
 
     zero = (0,) * len(digits)
-    gathers = [
-        Gather(me, lambda b: odir.at[b], order_b, g_send.at[1], g_recv.at[3]),
-        Gather(me, lambda b: vdir.at[b], order_a, g_send.at[0], g_recv.at[2]),
-    ]
-    odir[me] = moments(scatter_o.summed(zero), of, os_, of_new, os_new)
-    gathers[0].forward(own_event(gathers[0]))
-    vdir[me] = moments(scatter_v.summed(zero), vf, vs, vf_new, vs_new)
-    gathers[1].forward(own_event(gathers[1]))
-    scatter_o.drain()
-    scatter_v.drain()
-    gather_all(gathers)
+    ways = ((order_a, order_d), (order_b, order_c))
+
+    def both(v_dst, o_dst, base):
+        def make(dst, h, order, i):
+            return Gather(me, lambda b: dst.at[b, h], order, slow, g_send.at[i], g_recv.at[base + i])
+        return (
+            [make(o_dst, h, ways[1][h % 2], cuts + h) for h in range(cuts)],
+            [make(v_dst, h, ways[0][h % 2], h) for h in range(cuts)],
+        )
+
+    gathers_o, gathers_v = both(vdir, odir, 2)
+    for h in range(cuts):
+        odir[me, h] = moments(scatters_o[h].summed(zero), h, of, os_, of_new, os_new)
+        gathers_o[h].forward(own_event(gathers_o[h]))
+    for h in range(cuts):
+        vdir[me, h] = moments(scatters_v[h].summed(zero), h, vf, vs, vf_new, vs_new)
+        gathers_v[h].forward(own_event(gathers_v[h]))
+    for sc in scatters_o + scatters_v:
+        sc.drain()
+    gather_all(gathers_o + gathers_v)
     v_dir = merged(vdir)
     o_dir = merged(odir)
     squares[0] = jnp.full(squares.shape[1:], jnp.sum(v_dir * v_dir) + jnp.sum(o_dir * o_dir), jnp.float32)
@@ -384,21 +416,22 @@
         total = total + squares[off]
     scale = (step_rate / jnp.sqrt(1.0 + total / total_size))[0:1, 0:1]
 
-    def update(weight, product, new, step, copy):
+    gathers_o, gathers_v = both(vcopy, ocopy, 2 + 2 * cuts)
+
+    def update(weight, product, new, step, copy, gathers):
         s = scale * product
         w = weight[...] - s
+        rows = copy.shape[2]
+        narrow = w.astype(jnp.bfloat16)
+        for h, g in enumerate(gathers):
+            copy[me, h] = narrow[h * rows:(h + 1) * rows, :]
+            g.forward(own_event(g))
         step[...] = s
         new[...] = w
-        copy[me] = w.astype(jnp.bfloat16)
-
-    gathers = [
-        Gather(me, lambda b: vcopy.at[b], order_a, g_send.at[0], g_recv.at[4]),
-        Gather(me, lambda b: ocopy.at[b], order_b, g_send.at[1], g_recv.at[5]),
-    ]
-    update(vw, v_sum, vnew, vstep, vcopy)
-    gathers[0].forward(own_event(gathers[0]))
-    update(ow, o_sum, onew, ostep, ocopy)
-    gather_all(gathers)
+
+    update(vw, v_sum, vnew, vstep, vcopy, gathers_v)
+    update(ow, o_sum, onew, ostep, ocopy, gathers_o)
+    gather_all(gathers_v + gathers_o)
 
 
 def store(*refs):
@@ -417,39 +450,40 @@
     o_cols = of.shape[1]
     total_size = float(n * r * m * (v_cols + o_cols))
     halves = 2 if m % 2 == 0 else 1
+    cuts = 2
     vmem = pl.BlockSpec(memory_space=pltpu.VMEM)
     hbm = pl.BlockSpec(memory_space=pltpu.HBM)
     anywhere = pl.BlockSpec(memory_space=pl.ANY)
     outs = (
         (vw.shape, f32), (ow.shape, f32), (vw.shape, f32), (ow.shape, f32),
-        ((n, *vw.shape), bf16), ((n, *ow.shape), bf16),
+        ((n, cuts, vw.shape[0] // cuts, v_cols), bf16), ((n, cuts, ow.shape[0] // cuts, o_cols), bf16),
         (vf.shape, f32), (vf.shape, f32), (of.shape, f32), (of.shape, f32),
     )
     dma = pltpu.SemaphoreType.DMA
-    big = (x, vc, mo, oc, vw, ow, vf, vs, of, os_)
+    big = (x, vc, mo, oc, vw, ow, vf, vs, of, os_, vb, ob)
     ways = 2 + sum(s - 1 for s, _ in split_digits(n)[:-1])
     res = pl.pallas_call(
         functools.partial(kernel, n, m, total_size),
         out_shape=tuple(pltpu.VMEM(s, d) for s, d in outs),
-        in_specs=[hbm] * 10 + [vmem] * 2,
+        in_specs=[hbm] * 12,
         out_specs=[vmem] * 10,
         scratch_shapes=[
             *[pltpu.VMEM(a.shape, a.dtype) for a in big],
             pltpu.VMEM((n, halves, vb.shape[0] // halves, vb.shape[1]), bf16),
             pltpu.VMEM((n, halves, ob.shape[0] // halves, ob.shape[1]), bf16),
-            pltpu.VMEM((n, r, v_cols), f32), pltpu.VMEM((n, r, o_cols), f32),
+            pltpu.VMEM((n, cuts, r // cuts, v_cols), f32), pltpu.VMEM((n, cuts, r // cuts, o_cols), f32),
             pltpu.VMEM((n * r, v_cols), f32), pltpu.VMEM((n * r, o_cols), f32),
-            pltpu.VMEM((n, r, v_cols), f32), pltpu.VMEM((n, r, o_cols), f32),
-            pltpu.VMEM((n, r, v_cols), f32), pltpu.VMEM((n, r, o_cols), f32),
-            pltpu.VMEM((n, r, v_cols), f32), pltpu.VMEM((n, r, o_cols), f32),
+            pltpu.VMEM((n, cuts, r // cuts, v_cols), f32), pltpu.VMEM((n, cuts, r // cuts, o_cols), f32),
+            pltpu.VMEM((n, cuts, r // cuts, v_cols), f32), pltpu.VMEM((n, cuts, r // cuts, o_cols), f32),
+            pltpu.VMEM((n, cuts, r // cuts, v_cols), f32), pltpu.VMEM((n, cuts, r // cuts, o_cols), f32),
             pltpu.VMEM((m, 8, 128), f32),
-            dma((10,)), dma((2, n, ways)), dma((6, n)), dma((2, n)), dma((2, n)), dma((m,)), dma((m,)),
-            dma((2, n)), dma((2, n)),
+            dma((12,)), dma((2 * cuts, n, ways)), dma((2 + 4 * cuts, n)), dma((2 * cuts, n)), dma((2 * cuts, n)),
+            dma((m,)), dma((m,)), dma((2, n)), dma((2, n)), dma((2, split_digits(n)[-1][0])),
         ],
         compiler_params=pltpu.CompilerParams(
             collective_id=0, has_side_effects=True, vmem_limit_bytes=36 * 1024 * 1024
         ),
-    )(*[pltpu.with_memory_space_constraint(a, pltpu.HBM) for a in big], vb, ob)
+    )(*[pltpu.with_memory_space_constraint(a, pltpu.HBM) for a in big])
     res = pl.pallas_call(
         store,
         out_shape=tuple(jax.ShapeDtypeStruct(s, d) for s, d in outs),

time: 110 us -> 105 us (0.955)
  Pallas kernels: 108 us -> 104 us
  local copies, waits for them, and re-layouts: 1.59 us -> 0 us
    pallas_call x1, Pallas kernels: 106 us -> 102 us  [local(): pl.pallas_call(functools.partial(kernel, n, m, total_size), out_shape=tup...]
    unnamed x4 -> x0, local copies, waits for them, and re-layouts: 1.59 us -> none
where the time goes in v3:
time: 105 us
  Pallas kernels  104 us (99%)
    pallas_call x1, Pallas kernels, local(): pl.pallas_call(functools.partial(kernel, n, m, total_size), out_shape=tup...  102 us
    pallas_call x1, Pallas kernels, local(): pl.pallas_call(store, out_shape=tuple((jax.ShapeDtypeStruct(s, d) for s,...  2.49 us

profile of v3, /device:TPU:0, one launch (start us, length us, event | category | flops | bytes accessed | tf_op | source)
XLA Modules:
  0.0 104.7 jit_solution(12295604653852492642)
XLA Ops:
  0.6 101.6 %shard_map.195 = (f32[128,512]{1,0:T(8,128)S(1)}, f32[64,1024]{1,0:T(8,128)S(1)}, f32[128,512]{1,0:T(8,128)S(1)}, f32[64,1024]{1,0:T(8,128)S(1)}, bf16[16,2,64,5...) custom-call(bf16[1024,2048]{1,0:T(8,128)(2,1)} %x_hbm.1, ...), custom_call_target="tpu_custom_call" | custom-call | tf_op jit(solution)/shard_map/pallas_call | solution.py:465
  102.2 2.5 %shard_map.196 = (f32[128,512]{1,0:T(8,128)}, f32[64,1024]{1,0:T(8,128)}, f32[128,512]{1,0:T(8,128)}, f32[64,1024]{1,0:T(8,128)}, bf16[16,2,64,512]{3,2,1,0:T(8,...) custom-call(f32[128,512]{1,0:T(8,128)S(1)} %get-tuple-element.30.ref, ...), custom_call_target="tpu_custom_call" | custom-call | tf_op jit(solution)/shard_map/pallas_call | solution.py:487

commit v4 on v3

--- a/solution.py
+++ b/solution.py
@@ -280,7 +280,7 @@
             device_id_type=pl.DeviceIdType.MESH,
         )
         peers += 1
-    for c in loads:
+    for c in loads[:2]:
         c.start()
     halves = vb_all.shape[1]
     loads[0].wait()
@@ -310,16 +310,21 @@
             c.start()
             handed.append((i, block, c))
 
-    gather_all([
+    gathers = [
         Gather(me, lambda b: vb_all.at[b, half], order_a, slow, g_send.at[0], g_recv.at[0], z_send.at[0]),
         Gather(me, lambda b: ob_all.at[b, half], order_b, slow, g_send.at[1], g_recv.at[1], z_send.at[1]),
-    ], share)
+    ]
+    for g in gathers:
+        g.forward(own_event(g))
+    gather_all(gathers, share)
+    for c in loads[2:]:
+        c.start()
     for i, block, c in handed:
         c.wait_send()
         hand(i, block, 1 - half).wait_recv()
 
     tokens = x_ref.shape[0]
-    tile = min(256, tokens)
+    tile = min(512, tokens)
     cuts, r = vpart.shape[1:3]
 
     def project(src, cot, basis, acc, part):

time: 105 us -> 104 us (level)
    pallas_call x1, Pallas kernels: 102 us -> 100 us  [local(): pl.pallas_call(functools.partial(kernel, n, m, total_size), out_shape=tup...]
where the time goes in v4:
time: 104 us
  Pallas kernels  103 us (99%)
    pallas_call x1, Pallas kernels, local(): pl.pallas_call(functools.partial(kernel, n, m, total_size), out_shape=tup...  100 us
    pallas_call x1, Pallas kernels, local(): pl.pallas_call(store, out_shape=tuple((jax.ShapeDtypeStruct(s, d) for s,...  2.49 us

profile of v4, /device:TPU:0, one launch (start us, length us, event | category | flops | bytes accessed | tf_op | source)
XLA Modules:
  0.0 103.6 jit_solution(5409812095728080778)
XLA Ops:
  0.6 100.4 %shard_map.195 = (f32[128,512]{1,0:T(8,128)S(1)}, f32[64,1024]{1,0:T(8,128)S(1)}, f32[128,512]{1,0:T(8,128)S(1)}, f32[64,1024]{1,0:T(8,128)S(1)}, bf16[16,2,64,5...) custom-call(bf16[1024,2048]{1,0:T(8,128)(2,1)} %x_hbm.1, ...), custom_call_target="tpu_custom_call" | custom-call | tf_op jit(solution)/shard_map/pallas_call | solution.py:470
  101.1 2.5 %shard_map.196 = (f32[128,512]{1,0:T(8,128)}, f32[64,1024]{1,0:T(8,128)}, f32[128,512]{1,0:T(8,128)}, f32[64,1024]{1,0:T(8,128)}, bf16[16,2,64,512]{3,2,1,0:T(8,...) custom-call(f32[128,512]{1,0:T(8,128)S(1)} %get-tuple-element.30.ref, ...), custom_call_target="tpu_custom_call" | custom-call | tf_op jit(solution)/shard_map/pallas_call | solution.py:492
